TPU v7x, 32 devices: a whole 2x2x4 slice. The times are simulated.
32 devices in a mesh: ep: 8 (over z, core), tp: 4 (over y, x).
Axes of the slice: x: 2, y: 2, z: 4, core: 2. Of those that a mesh axis runs over, the one named last changes fastest.
Arguments:
- tokens: bfloat16 [1024, 2048], P('ep'), may hold values from -6 to 6
- chosen: int32 [8, 8, 8], replicated, may hold values from 0 to 127, as said below
- chosen_weight: float32 [8, 8, 8], P('ep'), may hold values from 0.1 to 1
- gate_weight: bfloat16 [8, 2048, 4096], P('ep', None, 'tp'), may hold values from -0.125 to 0.125
- up_weight: bfloat16 [8, 2048, 4096], P('ep', None, 'tp'), may hold values from -0.125 to 0.125
- down_weight: bfloat16 [8, 4096, 2048], P('ep', 'tp'), may hold values from -0.09375 to 0.09375
Outputs:
- combined: bfloat16 [1024, 2048], P('ep', 'tp')
Inputs may be any that keep to these rules, and one draw needn't show every extreme that they name: `chosen`: for every block and expert the 8 positions are distinct.
All inputs are finite; a program needn't handle non-finite values.
Results may differ from a plain program's by a relative error of at most 0.015.
Values may be sent and summed in bfloat16 or wider, within the bound.
A program may use at most 64 MiB of HBM per device.

v0:
```python
import functools

import jax
import jax.numpy as jnp
from jax import lax
from jax.experimental import pallas as pl
from jax.experimental.pallas import tpu as pltpu
from jax.sharding import PartitionSpec as P

MESH = pl.DeviceIdType.MESH
CHUNKS = 2


def each(count, body):
    if count <= 8:
        for i in range(count):
            body(i)
    else:
        pl.loop(0, count)(body)


def partner(t, j, count):
    if count & (count - 1):
        return lax.rem(t + j, count)
    out, bit = 0, 1
    while bit < count:
        have = (t // bit) % 2
        out = out + ((have + 1) % 2 if j & bit else have) * bit
        bit *= 2
    return out


def kernel(
    n_ep, n_tp,
    tok_hbm, cho_hbm, wt_hbm, gate_hbm, up_hbm, down_hbm,
    out_ref,
    tok, cho, wt, gate, up, down,
    leaving, arrived, gate_acc, up_acc, place,
    part_out, part_in, back_out, back_in,
    in_sem, w_sem, d_sem,
    s1_send, s1_recv, s2_send, s2_recv, s3_send, s3_recv,
):
    e = lax.axis_index("ep")
    t = lax.axis_index("tp")
    tok_count, width = tok.shape
    experts, picks = cho.shape
    rows = experts * picks
    cw = width // CHUNKS
    sw = width // n_tp
    half = n_ep // 2
    far = jnp.where(e < half, 1, 0)

    def ep_peer(j):
        low = n_ep - 1 - j
        low = jnp.where(low > e, low, low - 1)
        high = jnp.where(j < e, j, j + 1)
        return jnp.where(e < half, low, high)

    barrier = pltpu.get_barrier_semaphore()

    def greet(j):
        pl.semaphore_signal(barrier, inc=1, device_id={"ep": ep_peer(j)}, device_id_type=MESH)

    each(n_ep - 1, greet)
    for j in range(1, n_tp):
        pl.semaphore_signal(
            barrier, inc=1, device_id={"tp": partner(t, j, n_tp)}, device_id_type=MESH
        )

    loads = [
        pltpu.make_async_copy(cho_hbm.at[e], cho, in_sem.at[0]),
        pltpu.make_async_copy(wt_hbm.at[0], wt, in_sem.at[1]),
        pltpu.make_async_copy(tok_hbm, tok, in_sem.at[2]),
    ]
    for c in loads:
        c.start()
    wloads = []
    for k in range(CHUNKS):
        piece = pl.ds(k * cw, cw)
        a = pltpu.make_async_copy(gate_hbm.at[0, piece, :], gate.at[piece, :], w_sem.at[0, k])
        b = pltpu.make_async_copy(up_hbm.at[0, piece, :], up.at[piece, :], w_sem.at[1, k])
        wloads.append((a, b))
    order = [*range(n_tp - 1, 0, -1), 0]
    dloads = {}
    for j in order:
        col = pl.multiple_of(partner(t, j, n_tp) * sw, sw)
        dloads[j] = pltpu.make_async_copy(
            down_hbm.at[0, :, pl.ds(col, sw)], down.at[j], d_sem.at[j]
        )

    for c in loads:
        c.wait()
    lane = lax.broadcasted_iota(jnp.int32, (picks, picks), 1)
    sub = lax.broadcasted_iota(jnp.int32, (picks, picks), 0)
    diag = lane == sub
    position = lax.broadcasted_iota(jnp.int32, (picks, tok_count), 1).astype(jnp.float32)
    hots, parts = [], []
    for x in range(experts):
        spread = jnp.broadcast_to(cho[x : x + 1, :], (picks, picks)).astype(jnp.float32)
        column = jnp.sum(jnp.where(diag, spread, 0.0), axis=1, keepdims=True)
        wide = jnp.broadcast_to(wt[x : x + 1, :], (picks, picks))
        wcol = jnp.sum(jnp.where(diag, wide, 0.0), axis=1, keepdims=True)
        hit = position == column
        hots.append(jnp.where(hit, 1.0, 0.0))
        parts.append(jnp.where(hit, wcol, 0.0))
    onehot = jnp.concatenate(hots, axis=0).astype(jnp.bfloat16)
    for k in range(CHUNKS):
        sel = jnp.dot(
            onehot, tok[:, k * cw : (k + 1) * cw], preferred_element_type=jnp.float32
        )
        leaving[k] = sel.reshape(experts, picks, cw).astype(jnp.bfloat16)

    pl.semaphore_wait(barrier, n_ep - 1 + n_tp - 1)

    def send_tokens(k, j):
        p = ep_peer(j)
        return pltpu.make_async_remote_copy(
            src_ref=leaving.at[k, p],
            dst_ref=arrived.at[k, e],
            send_sem=s1_send.at[k, j],
            recv_sem=s1_recv.at[k, e],
            device_id={"ep": p},
            device_id_type=MESH,
        )

    for k in range(CHUNKS):
        each(n_ep - 1, lambda j: send_tokens(k, j).start())
    for a, b in wloads:
        a.start()
        b.start()
    for j in order:
        dloads[j].start()

    weighted = jnp.concatenate(parts, axis=0)
    hi = weighted.astype(jnp.bfloat16).astype(jnp.float32)
    mid = (weighted - hi).astype(jnp.bfloat16).astype(jnp.float32)
    lo = weighted - hi - mid
    for i, piece in enumerate((hi, mid, lo)):
        place[i] = piece.T.astype(jnp.bfloat16)

    def rows_in(ref, k, sem, p):
        pltpu.make_async_remote_copy(
            src_ref=ref.at[k, p] if k is not None else ref.at[p],
            dst_ref=ref.at[k, p] if k is not None else ref.at[p],
            send_sem=sem.at[k, p] if k is not None else sem.at[p],
            recv_sem=sem.at[k, p] if k is not None else sem.at[p],
            device_id={"ep": p},
            device_id_type=MESH,
        ).wait_recv()

    for k in range(CHUNKS):
        arrived[k, e] = leaving[k, e]
        each(n_ep - 1, lambda j: rows_in(arrived, k, s1_recv, ep_peer(j)))
        x = arrived[k].astype(jnp.float32).reshape(rows, cw).astype(jnp.bfloat16)
        for c in wloads[k]:
            c.wait()
        g = jnp.dot(x, gate[k * cw : (k + 1) * cw, :], preferred_element_type=jnp.float32)
        u = jnp.dot(x, up[k * cw : (k + 1) * cw, :], preferred_element_type=jnp.float32)
        if k == 0:
            gate_acc[...] = g
            up_acc[...] = u
        else:
            gate_acc[...] += g
            up_acc[...] += u
    g = gate_acc[...]
    hidden = (g / (1.0 + jnp.exp(-g)) * up_acc[...]).astype(jnp.bfloat16)

    def send_part(h, j):
        side = far if h == 0 else 1 - far
        return pltpu.make_async_remote_copy(
            src_ref=part_out.at[j, side],
            dst_ref=part_in.at[j - 1, side],
            send_sem=s2_send.at[h, j],
            recv_sem=s2_recv.at[h, j],
            device_id={"tp": partner(t, j, n_tp)},
            device_id_type=MESH,
        )

    def send_back(j):
        p = ep_peer(j)
        return pltpu.make_async_remote_copy(
            src_ref=back_out.at[p],
            dst_ref=back_in.at[e],
            send_sem=s3_send.at[j],
            recv_sem=s3_recv.at[e],
            device_id={"ep": p},
            device_id_type=MESH,
        )

    for j in order:
        dloads[j].wait()
        part = jnp.dot(hidden, down[j], preferred_element_type=jnp.float32)
        part_out[j] = part.reshape(2, rows // 2, sw).astype(jnp.bfloat16)
        if j:
            send_part(0, j).start()
            send_part(1, j).start()
    for h in range(2):
        side = far if h == 0 else 1 - far
        total = part_out[0, side].astype(jnp.float32)
        for j in range(n_tp - 1, 0, -1):
            send_part(h, j).wait_recv()
            total += part_in[j - 1, side].astype(jnp.float32)
        back_out[pl.ds(side * half, half)] = total.reshape(half, picks, sw).astype(jnp.bfloat16)
        if h == 0:
            each(half, lambda j: send_back(j).start())
        else:
            each(half - 1, lambda j: send_back(j + half).start())
    back_in[e] = back_out[e]
    each(n_ep - 1, lambda j: rows_in(back_in, None, s3_recv, ep_peer(j)))
    y = back_in[...].astype(jnp.float32).reshape(rows, sw).astype(jnp.bfloat16)
    terms = jnp.concatenate([place[0], place[1], place[2]], axis=0)
    terms = jnp.dot(terms, y, preferred_element_type=jnp.float32)
    result = terms[:tok_count] + terms[tok_count : 2 * tok_count] + terms[2 * tok_count :]
    out_ref[...] = result.astype(out_ref.dtype)

    for k in range(CHUNKS):
        each(n_ep - 1, lambda j: send_tokens(k, j).wait_send())
    for j in range(1, n_tp):
        send_part(0, j).wait_send()
        send_part(1, j).wait_send()
    each(n_ep - 1, lambda j: send_back(j).wait_send())


def local(tokens, chosen, chosen_weight, gate_weight, up_weight, down_weight):
    n_ep, n_tp = lax.axis_size("ep"), lax.axis_size("tp")
    tok_count, width = tokens.shape
    blocks, experts, picks = chosen.shape
    hid = gate_weight.shape[2]
    rows = blocks * picks
    cw, sw = width // CHUNKS, width // n_tp
    bf, f32 = jnp.bfloat16, jnp.float32
    dma = pltpu.SemaphoreType.DMA
    hbm = pl.BlockSpec(memory_space=pltpu.HBM)
    return pl.pallas_call(
        functools.partial(kernel, n_ep, n_tp),
        out_shape=jax.ShapeDtypeStruct((tok_count, sw), bf),
        in_specs=[hbm] * 6,
        out_specs=pl.BlockSpec(memory_space=pltpu.VMEM),
        scratch_shapes=[
            pltpu.VMEM((tok_count, width), bf),
            pltpu.VMEM((experts, picks), jnp.int32),
            pltpu.VMEM((experts, picks), f32),
            pltpu.VMEM((width, hid), bf),
            pltpu.VMEM((width, hid), bf),
            pltpu.VMEM((n_tp, hid, sw), bf),
            pltpu.VMEM((CHUNKS, experts, picks, cw), bf),
            pltpu.VMEM((CHUNKS, blocks, picks, cw), bf),
            pltpu.VMEM((rows, hid), f32),
            pltpu.VMEM((rows, hid), f32),
            pltpu.VMEM((3, tok_count, experts * picks), bf),
            pltpu.VMEM((n_tp, 2, rows // 2, sw), bf),
            pltpu.VMEM((n_tp - 1, 2, rows // 2, sw), bf),
            pltpu.VMEM((blocks, picks, sw), bf),
            pltpu.VMEM((experts, picks, sw), bf),
            dma((3,)),
            dma((2, CHUNKS)),
            dma((n_tp,)),
            dma((CHUNKS, n_ep)),
            dma((CHUNKS, n_ep)),
            dma((2, n_tp)),
            dma((2, n_tp)),
            dma((n_ep,)),
            dma((n_ep,)),
        ],
        compiler_params=pltpu.CompilerParams(
            collective_id=0, has_side_effects=True, vmem_limit_bytes=32 * 1024 * 1024
        ),
    )(*(
        pltpu.with_memory_space_constraint(a, pltpu.HBM)
        for a in (tokens, chosen, chosen_weight, gate_weight, up_weight, down_weight)
    ))


def solution(mesh):
    return jax.shard_map(
        local,
        mesh=mesh,
        in_specs=(
            P("ep", None),
            P(),
            P("ep", None, None),
            P("ep", None, "tp"),
            P("ep", None, "tp"),
            P("ep", "tp", None),
        ),
        out_specs=P("ep", "tp"),
        check_vma=False,
    )
```

profile of v0, /device:TPU:0, one launch (start us, length us, event | category | flops | bytes accessed | tf_op | source)
XLA Modules:
  0.0 23.3 jit_solution(13675108544541042495)
XLA Ops:
  0.0 22.7 %shard_map.64 = bf16[128,512]{1,0:T(8,128)(2,1)S(1)} custom-call(bf16[128,2048]{1,0:T(8,128)(2,1)} %tok_hbm.1, s32[8,8,8]{2,1,0:T(8,128)} %cho_hbm.1, f32[1,8,8]{2,1,0:T(8,128)} %wt_hbm.1, bf16[1,2048,1024]{2,1,0:T(8,128)(2,1)} %gate_hbm.1, bf16[1,2048,1024]{2,1,0:T(8,128)(2,1)} %up_hbm.1, bf16[1,1024,2048]{2,1,0:T(8,128)(2,1)} %down_hbm.1), custom_call_target="tpu_custom_call" | custom-call | tf_op jit(solution)/shard_map/pallas_call | solution.py:234
  22.7 0.7 %copy.8 = bf16[128,512]{1,0:T(8,128)(2,1)} copy(bf16[128,512]{1,0:T(8,128)(2,1)S(1)} %shard_map.64) | data formatting | bytes 262144
where the time goes:
time: 23.5 us; the launch traced here: 23.3 us
  Pallas kernels  22.7 us (97%)
  local copies, waits for them, and re-layouts  0.66 us (3%)
    pallas_call x1, Pallas kernels, local(): pl.pallas_call(functools.partial(kernel, n_ep, n_tp), out_shape=jax.Shape...  22.7 us
    unnamed x1, local copies, waits for them, and re-layouts  0.66 us

commit v1 on v0

v1 whole, which is shorter than its diff:
```python
import functools

import jax
import jax.numpy as jnp
from jax import lax
from jax.experimental import pallas as pl
from jax.experimental.pallas import tpu as pltpu
from jax.sharding import PartitionSpec as P

MESH = pl.DeviceIdType.MESH
GROUPS = 4
EARLY = 2


def each(count, body):
    if count <= 8:
        for i in range(count):
            body(i)
    else:
        pl.loop(0, count)(body)


def kernel(
    n_ep, n_tp,
    tok_hbm, cho_hbm, wt_hbm, gate_hbm, up_hbm, down_hbm,
    out_ref,
    tok, cho, wt, gate, up, down,
    leaving, arrived, gate_acc, up_acc, place,
    part_out, part_in, back_out, back_in,
    in_sem, w_sem, d_sem,
    s1_send, s1_recv, hop_send, hop_recv, fan_send, fan_recv, s2_send, s2_recv, s3_send, s3_recv,
    ep_ready, tp_ready,
):
    e = lax.axis_index("ep")
    t = lax.axis_index("tp")
    tok_count, width = tok.shape
    experts, picks = cho.shape
    rows = experts * picks
    sw = width // n_tp
    gs = n_ep // GROUPS
    mine = e // gs

    def group_at(i):
        if i == GROUPS - 1:
            return mine
        low = GROUPS - 1 - i
        low = jnp.where(low > mine, low, low - 1)
        high = jnp.where(i < mine, i, i + 1)
        return jnp.where(mine < GROUPS // 2, low, high)

    def quarter_at(i):
        if i == n_tp - 1:
            return t
        down_first = n_tp - 1 - i
        up_first = jnp.where(i < t, i, i + 1)
        return jnp.where(t == 0, down_first, up_first)

    barrier = pltpu.get_barrier_semaphore()

    def greet(p):
        pl.semaphore_signal(barrier, inc=1, device_id={"ep": p}, device_id_type=MESH)

    pl.loop(e + 1, n_ep)(greet)

    def greet_tp(p):
        pl.semaphore_signal(barrier, inc=1, device_id={"tp": p}, device_id_type=MESH)

    pl.loop(t + 1, n_tp)(greet_tp)

    loads = [
        pltpu.make_async_copy(cho_hbm.at[e], cho, in_sem.at[0]),
        pltpu.make_async_copy(wt_hbm.at[0], wt, in_sem.at[1]),
        pltpu.make_async_copy(tok_hbm, tok, in_sem.at[2]),
    ]
    for c in loads:
        c.start()
    wloads = []
    for k in range(n_tp):
        piece = pl.ds(k * sw, sw)
        a = pltpu.make_async_copy(gate_hbm.at[0, piece, :], gate.at[piece, :], w_sem.at[0, k])
        b = pltpu.make_async_copy(up_hbm.at[0, piece, :], up.at[piece, :], w_sem.at[1, k])
        wloads.append((a, b))
    dloads = []
    for i in range(n_tp):
        col = pl.multiple_of(quarter_at(i) * sw, sw)
        dloads.append(
            pltpu.make_async_copy(down_hbm.at[0, :, pl.ds(col, sw)], down.at[i], d_sem.at[i])
        )

    with jax.named_scope("barrier"):
        @pl.when(e + t > 0)
        def _():
            pl.semaphore_wait(barrier, e + t)

    def answer(p):
        pl.semaphore_signal(ep_ready.at[e], inc=1, device_id={"ep": p}, device_id_type=MESH)

    pl.loop(0, e)(answer)

    def answer_tp(p):
        pl.semaphore_signal(tp_ready, inc=1, device_id={"tp": p}, device_id_type=MESH)

    pl.loop(0, t)(answer_tp)

    with jax.named_scope("loadwait"):
        for c in loads:
            c.wait()
    for a, b in wloads:
        a.start()
        b.start()
    for c in dloads:
        c.start()

    lane = lax.broadcasted_iota(jnp.int32, (picks, picks), 1)
    sub = lax.broadcasted_iota(jnp.int32, (picks, picks), 0)
    diag = lane == sub
    position = lax.broadcasted_iota(jnp.int32, (picks, tok_count), 1).astype(jnp.float32)
    columns, hots = [], []
    for x in range(experts):
        spread = jnp.broadcast_to(cho[x : x + 1, :], (picks, picks)).astype(jnp.float32)
        column = jnp.sum(jnp.where(diag, spread, 0.0), axis=1, keepdims=True)
        columns.append(column)
        hots.append(jnp.where(position == column, 1.0, 0.0))
    onehot = jnp.concatenate(hots, axis=0).astype(jnp.bfloat16)
    with jax.named_scope("gather"):
        for k in range(n_tp):
            sel = jnp.dot(
                onehot, tok[:, k * sw : (k + 1) * sw], preferred_element_type=jnp.float32
            )
            leaving[k] = sel.reshape(experts, picks, sw).astype(jnp.bfloat16)

    def send_tokens(k, p):
        return pltpu.make_async_remote_copy(
            src_ref=leaving.at[k, p],
            dst_ref=arrived.at[k, e],
            send_sem=s1_send,
            recv_sem=s1_recv.at[k],
            device_id={"ep": p},
            device_id_type=MESH,
        )

    def send_hop(p):
        return pltpu.make_async_remote_copy(
            src_ref=leaving.at[t, p],
            dst_ref=arrived.at[t, e],
            send_sem=hop_send,
            recv_sem=hop_recv,
            device_id={"ep": p},
            device_id_type=MESH,
        )

    def send_group(g):
        for k in range(n_tp):
            each(gs, lambda i: send_tokens(k, g * gs + i).start())

    def ready_group(g):
        each(gs, lambda i: pl.semaphore_wait(ep_ready.at[g * gs + i], 1))

    with jax.named_scope("senddown"):
        pl.loop(0, mine)(send_group)

        def send_near(i):
            p = mine * gs + i

            @pl.when(p > e)
            def _():
                pl.semaphore_wait(ep_ready.at[p], 1)

            @pl.when(p != e)
            def _():
                for k in range(n_tp):
                    send_tokens(k, p).start()

        each(gs, send_near)
    with jax.named_scope("sendup"):
        @pl.when(mine < GROUPS - 1)
        def _():
            ready_group(mine + 1)
            each(gs, lambda i: send_hop((mine + 1) * gs + i).start())

        def send_up(g):
            ready_group(g)
            send_group(g)

        pl.loop(mine + 2, GROUPS)(send_up)

    parts = []
    for x in range(experts):
        wide = jnp.broadcast_to(wt[x : x + 1, :], (picks, picks))
        wcol = jnp.sum(jnp.where(diag, wide, 0.0), axis=1, keepdims=True)
        parts.append(jnp.where(position == columns[x], wcol, 0.0))
    weighted = jnp.concatenate(parts, axis=0)
    hi = weighted.astype(jnp.bfloat16).astype(jnp.float32)
    mid = (weighted - hi).astype(jnp.bfloat16).astype(jnp.float32)
    lo = weighted - hi - mid
    place[...] = jnp.concatenate([hi, mid, lo], axis=0).T.astype(jnp.bfloat16)

    def landed(ref, sem):
        pltpu.make_async_copy(ref, ref, sem).wait()


    @pl.when(t < n_tp - 1)
    def _():
        pl.semaphore_wait(tp_ready, n_tp - 1 - t)

    below = pl.ds((mine - 1) * gs, gs)

    def send_fan(i):
        return pltpu.make_async_remote_copy(
            src_ref=arrived.at[t, below],
            dst_ref=arrived.at[t, below],
            send_sem=fan_send,
            recv_sem=fan_recv.at[t],
            device_id={"tp": quarter_at(i)},
            device_id_type=MESH,
        )

    with jax.named_scope("fan"):
        @pl.when(mine > 0)
        def _():
            landed(arrived.at[t, pl.ds(0, gs)], hop_recv)
            for i in range(n_tp - 1):
                send_fan(i).start()

    for k in range(n_tp):
        arrived[k, e] = leaving[k, e]

        with jax.named_scope(f'tokin#k={k}'):
            @pl.when(mine == 0)
            def _():
                landed(arrived.at[k, pl.ds(0, n_ep - 1)], s1_recv.at[k])

            @pl.when(mine > 0)
            def _():
                landed(arrived.at[k, pl.ds(0, n_ep - 1 - gs)], s1_recv.at[k])

            @pl.when(jnp.logical_and(mine > 0, t != k))
            def _():
                landed(arrived.at[k, pl.ds(0, gs)], fan_recv.at[k])

        x = arrived[k].astype(jnp.float32).reshape(rows, sw).astype(jnp.bfloat16)
        for c in wloads[k]:
            c.wait()
        g = jnp.dot(x, gate[k * sw : (k + 1) * sw, :], preferred_element_type=jnp.float32)
        u = jnp.dot(x, up[k * sw : (k + 1) * sw, :], preferred_element_type=jnp.float32)
        if k == 0:
            gate_acc[...] = g
            up_acc[...] = u
        elif k < n_tp - 1:
            gate_acc[...] += g
            up_acc[...] += u
    g = gate_acc[...] + g
    u = up_acc[...] + u
    with jax.named_scope("hidden"):
        hidden = (g / (1.0 + jnp.exp(-g)) * u).astype(jnp.bfloat16)

    def send_part(i, gi):
        blocks = pl.ds(group_at(gi) * gs, gs)
        return pltpu.make_async_remote_copy(
            src_ref=part_out.at[i, blocks],
            dst_ref=part_in.at[t, blocks],
            send_sem=s2_send,
            recv_sem=s2_recv.at[gi],
            device_id={"tp": quarter_at(i)},
            device_id_type=MESH,
        )

    def send_back(p):
        return pltpu.make_async_remote_copy(
            src_ref=back_out.at[p],
            dst_ref=back_in.at[e],
            send_sem=s3_send,
            recv_sem=s3_recv,
            device_id={"ep": p},
            device_id_type=MESH,
        )

    for i in range(n_tp):
        dloads[i].wait()
        with jax.named_scope(f'down#i={i}'):
            part = jnp.dot(hidden, down[i], preferred_element_type=jnp.float32)
            part_out[i] = part.reshape(experts, picks, sw).astype(jnp.bfloat16)
        if i < n_tp - 1:
            for gi in range(EARLY):
                send_part(i, gi).start()
        if i == n_tp - 2:
            for gi in range(EARLY, GROUPS):
                for x in range(n_tp - 1):
                    send_part(x, gi).start()
    for gi in range(GROUPS):
        gg = group_at(gi)
        total = part_out[n_tp - 1, pl.ds(gg * gs, gs)].astype(jnp.float32)
        with jax.named_scope(f'rs#g={gi}'):
            landed(part_in.at[pl.ds(0, n_tp - 1), pl.ds(gg * gs, gs)], s2_recv.at[gi])
        for i in range(n_tp - 1):
            total += part_in[quarter_at(i), pl.ds(gg * gs, gs)].astype(jnp.float32)
        back_out[pl.ds(gg * gs, gs)] = total.astype(jnp.bfloat16)

        def give(i):
            p = gg * gs + i
            if gi < GROUPS - 1:
                send_back(p).start()
            else:
                @pl.when(p != e)
                def _():
                    send_back(p).start()

        each(gs, give)
    back_in[e] = back_out[e]

    with jax.named_scope('backin'):
        landed(back_in.at[pl.ds(0, n_ep - 1)], s3_recv)
    with jax.named_scope("combine"):
        y = back_in[...].astype(jnp.float32).reshape(rows, sw).astype(jnp.bfloat16)
        y = jnp.concatenate([y, y, y], axis=0)
        result = jnp.dot(place[...], y, preferred_element_type=jnp.float32)
        out_ref[...] = result.astype(out_ref.dtype)

    with jax.named_scope("drain"):
        for k in range(n_tp):
            @pl.when(mine == GROUPS - 1)
            def _():
                landed(leaving.at[k, pl.ds(0, n_ep - 1)], s1_send)

            @pl.when(mine < GROUPS - 1)
            def _():
                landed(leaving.at[k, pl.ds(0, n_ep - 1 - gs)], s1_send)

        @pl.when(mine < GROUPS - 1)
        def _():
            landed(leaving.at[0, pl.ds(0, gs)], hop_send)

        @pl.when(mine > 0)
        def _():
            landed(arrived.at[pl.ds(0, n_tp - 1), pl.ds(0, gs)], fan_send)

        landed(part_out.at[pl.ds(0, n_tp - 1)], s2_send)
        landed(back_out.at[pl.ds(0, n_ep - 1)], s3_send)


def local(tokens, chosen, chosen_weight, gate_weight, up_weight, down_weight):
    n_ep, n_tp = lax.axis_size("ep"), lax.axis_size("tp")
    tok_count, width = tokens.shape
    blocks, experts, picks = chosen.shape
    hid = gate_weight.shape[2]
    rows = blocks * picks
    sw = width // n_tp
    bf, f32 = jnp.bfloat16, jnp.float32
    dma = pltpu.SemaphoreType.DMA
    hbm = pl.BlockSpec(memory_space=pltpu.HBM)
    return pl.pallas_call(
        functools.partial(kernel, n_ep, n_tp),
        out_shape=jax.ShapeDtypeStruct((tok_count, sw), bf),
        in_specs=[hbm] * 6,
        out_specs=pl.BlockSpec(memory_space=pltpu.VMEM),
        scratch_shapes=[
            pltpu.VMEM((tok_count, width), bf),
            pltpu.VMEM((experts, picks), jnp.int32),
            pltpu.VMEM((experts, picks), f32),
            pltpu.VMEM((width, hid), bf),
            pltpu.VMEM((width, hid), bf),
            pltpu.VMEM((n_tp, hid, sw), bf),
            pltpu.VMEM((n_tp, experts, picks, sw), bf),
            pltpu.VMEM((n_tp, blocks, picks, sw), bf),
            pltpu.VMEM((rows, hid), f32),
            pltpu.VMEM((rows, hid), f32),
            pltpu.VMEM((tok_count, 3 * experts * picks), bf),
            pltpu.VMEM((n_tp, blocks, picks, sw), bf),
            pltpu.VMEM((n_tp, blocks, picks, sw), bf),
            pltpu.VMEM((blocks, picks, sw), bf),
            pltpu.VMEM((experts, picks, sw), bf),
            dma((3,)),
            dma((2, n_tp)),
            dma((n_tp,)),
            dma,
            dma((n_tp,)),
            dma,
            dma,
            dma,
            dma((n_tp,)),
            dma,
            dma((GROUPS,)),
            dma,
            dma,
            pltpu.SemaphoreType.REGULAR((n_ep,)),
            pltpu.SemaphoreType.REGULAR,
        ],
        compiler_params=pltpu.CompilerParams(
            collective_id=0, has_side_effects=True, vmem_limit_bytes=32 * 1024 * 1024
        ),
    )(*(
        pltpu.with_memory_space_constraint(a, pltpu.HBM)
        for a in (tokens, chosen, chosen_weight, gate_weight, up_weight, down_weight)
    ))


def solution(mesh):
    return jax.shard_map(
        local,
        mesh=mesh,
        in_specs=(
            P("ep", None),
            P(),
            P("ep", None, None),
            P("ep", None, "tp"),
            P("ep", None, "tp"),
            P("ep", "tp", None),
        ),
        out_specs=P("ep", "tp"),
        check_vma=False,
    )
```

time: 23.5 us -> 22.4 us (0.953)
  Pallas kernels: 22.7 us -> 21.5 us
    pallas_call x1, Pallas kernels: 22.7 us -> 21.5 us  [local(): pl.pallas_call(functools.partial(kernel, n_ep, n_tp), out_shape=jax.Shape...]
where the time goes in v1:
time: 22.4 us; the launch traced here: 22.2 us
  Pallas kernels  21.5 us (96%)
  local copies, waits for them, and re-layouts  0.66 us (3%)
    pallas_call x1, Pallas kernels, local(): pl.pallas_call(functools.partial(kernel, n_ep, n_tp), out_shape=jax.Shape...  21.5 us
    unnamed x1, local copies, waits for them, and re-layouts  0.66 us

profile of v1, /device:TPU:0, one launch (start us, length us, event | category | flops | bytes accessed | tf_op | source)
XLA Modules:
  0.0 22.2 jit_solution(17972710876205797456)
XLA Ops:
  0.0 21.5 %shard_map.64 = bf16[128,512]{1,0:T(8,128)(2,1)S(1)} custom-call(bf16[128,2048]{1,0:T(8,128)(2,1)} %tok_hbm.1, s32[8,8,8]{2,1,0:T(8,128)} %cho_hbm.1, f32[1,8,8]{2,1,0:T(8,128)} %wt_hbm.1, bf16[1,2048,1024]{2,1,0:T(8,128)(2,1)} %gate_hbm.1, bf16[1,2048,1024]{2,1,0:T(8,128)(2,1)} %up_hbm.1, bf16[1,1024,2048]{2,1,0:T(8,128)(2,1)} %down_hbm.1), custom_call_target="tpu_custom_call" | custom-call | tf_op jit(solution)/shard_map/pallas_call | solution.py:351
  21.5 0.7 %copy.8 = bf16[128,512]{1,0:T(8,128)(2,1)} copy(bf16[128,512]{1,0:T(8,128)(2,1)S(1)} %shard_map.64) | data formatting | bytes 262144

commit v2 on v1

--- a/solution.py
+++ b/solution.py
@@ -9,6 +9,8 @@
 
 MESH = pl.DeviceIdType.MESH
 GROUPS = 4
+COLUMNS = 4
+FAR = 2
 EARLY = 2
 
 
@@ -26,10 +28,10 @@
     out_ref,
     tok, cho, wt, gate, up, down,
     leaving, arrived, gate_acc, up_acc, place,
-    part_out, part_in, back_out, back_in,
+    part_out, part_in, first_in, back_out, back_in,
     in_sem, w_sem, d_sem,
-    s1_send, s1_recv, hop_send, hop_recv, fan_send, fan_recv, s2_send, s2_recv, s3_send, s3_recv,
-    ep_ready, tp_ready,
+    s1_send, s1_recv, hop_send, hop_recv, fan_send, fan_recv, s2_send, s2_recv, s3_send, s3_recv, first_send, first_recv,
+    ep_ready, tp_seen, tp_ready,
 ):
     e = lax.axis_index("ep")
     t = lax.axis_index("tp")
@@ -43,10 +45,16 @@
     def group_at(i):
         if i == GROUPS - 1:
             return mine
-        low = GROUPS - 1 - i
-        low = jnp.where(low > mine, low, low - 1)
-        high = jnp.where(i < mine, i, i + 1)
-        return jnp.where(mine < GROUPS // 2, low, high)
+        top = GROUPS - 1 - i
+        down = GROUPS - i
+        down = jnp.where(down > mine, down, down - 1) if i else 0
+        up = jnp.where(i < mine, i, i + 1)
+        return jnp.where(mine == 0, top, jnp.where(mine < GROUPS // 2, down, up))
+
+    def direct(src, dst):
+        return jnp.logical_or(
+            jnp.logical_and(dst == 0, src >= FAR), jnp.logical_and(src == 0, dst > 0)
+        )
 
     def quarter_at(i):
         if i == n_tp - 1:
@@ -65,7 +73,9 @@
     def greet_tp(p):
         pl.semaphore_signal(barrier, inc=1, device_id={"tp": p}, device_id_type=MESH)
 
-    pl.loop(t + 1, n_tp)(greet_tp)
+    @pl.when(t == 0)
+    def _():
+        pl.loop(1, n_tp)(greet_tp)
 
     loads = [
         pltpu.make_async_copy(cho_hbm.at[e], cho, in_sem.at[0]),
@@ -88,19 +98,21 @@
         )
 
     with jax.named_scope("barrier"):
-        @pl.when(e + t > 0)
-        def _():
-            pl.semaphore_wait(barrier, e + t)
+        floor = e + jnp.minimum(t, 1)
+
+        @pl.when(floor > 0)
+        def _():
+            pl.semaphore_wait(barrier, floor)
+
 
     def answer(p):
         pl.semaphore_signal(ep_ready.at[e], inc=1, device_id={"ep": p}, device_id_type=MESH)
 
     pl.loop(0, e)(answer)
 
-    def answer_tp(p):
-        pl.semaphore_signal(tp_ready, inc=1, device_id={"tp": p}, device_id_type=MESH)
-
-    pl.loop(0, t)(answer_tp)
+    @pl.when(t > 0)
+    def _():
+        pl.semaphore_signal(tp_seen, inc=1, device_id={"tp": 0}, device_id_type=MESH)
 
     with jax.named_scope("loadwait"):
         for c in loads:
@@ -172,12 +184,23 @@
                     send_tokens(k, p).start()
 
         each(gs, send_near)
-    with jax.named_scope("sendup"):
+    with jax.named_scope("hop"):
         @pl.when(mine < GROUPS - 1)
         def _():
             ready_group(mine + 1)
             each(gs, lambda i: send_hop((mine + 1) * gs + i).start())
 
+    with jax.named_scope("tpseen"):
+        @pl.when(t == 0)
+        def _():
+            pl.semaphore_wait(tp_seen, n_tp - 1)
+
+            def admit(p):
+                pl.semaphore_signal(tp_ready, inc=1, device_id={"tp": p}, device_id_type=MESH)
+
+            pl.loop(1, n_tp)(admit)
+
+    with jax.named_scope("sendup"):
         def send_up(g):
             ready_group(g)
             send_group(g)
@@ -199,9 +222,9 @@
         pltpu.make_async_copy(ref, ref, sem).wait()
 
 
-    @pl.when(t < n_tp - 1)
+    @pl.when(t > 0)
     def _():
-        pl.semaphore_wait(tp_ready, n_tp - 1 - t)
+        pl.semaphore_wait(tp_ready, 1)
 
     below = pl.ds((mine - 1) * gs, gs)
 
@@ -224,7 +247,15 @@
 
     for k in range(n_tp):
         arrived[k, e] = leaving[k, e]
-
+    for a, b in wloads:
+        a.wait()
+        b.wait()
+    for c in dloads:
+        c.wait()
+    hid = gate.shape[1]
+    step = hid // COLUMNS
+    hidden = []
+    for k in range(n_tp):
         with jax.named_scope(f'tokin#k={k}'):
             @pl.when(mine == 0)
             def _():
@@ -239,20 +270,19 @@
                 landed(arrived.at[k, pl.ds(0, gs)], fan_recv.at[k])
 
         x = arrived[k].astype(jnp.float32).reshape(rows, sw).astype(jnp.bfloat16)
-        for c in wloads[k]:
-            c.wait()
-        g = jnp.dot(x, gate[k * sw : (k + 1) * sw, :], preferred_element_type=jnp.float32)
-        u = jnp.dot(x, up[k * sw : (k + 1) * sw, :], preferred_element_type=jnp.float32)
-        if k == 0:
-            gate_acc[...] = g
-            up_acc[...] = u
-        elif k < n_tp - 1:
-            gate_acc[...] += g
-            up_acc[...] += u
-    g = gate_acc[...] + g
-    u = up_acc[...] + u
-    with jax.named_scope("hidden"):
-        hidden = (g / (1.0 + jnp.exp(-g)) * u).astype(jnp.bfloat16)
+        deep = pl.ds(k * sw, sw)
+        for c in range(COLUMNS):
+            cols = pl.ds(c * step, step)
+            g = jnp.dot(x, gate[deep, cols], preferred_element_type=jnp.float32)
+            u = jnp.dot(x, up[deep, cols], preferred_element_type=jnp.float32)
+            if k > 0:
+                g += gate_acc[:, cols]
+                u += up_acc[:, cols]
+            if k < n_tp - 1:
+                gate_acc[:, cols] = g
+                up_acc[:, cols] = u
+            else:
+                hidden.append((g / (1.0 + jnp.exp(-g)) * u).astype(jnp.bfloat16))
 
     def send_part(i, gi):
         blocks = pl.ds(group_at(gi) * gs, gs)
@@ -265,6 +295,33 @@
             device_id_type=MESH,
         )
 
+    def start_part(i, gi):
+        if i > 0:
+            send_part(i, gi).start()
+        else:
+            @pl.when(jnp.logical_or(t == 0, jnp.logical_not(direct(mine, group_at(gi)))))
+            def _():
+                send_part(i, gi).start()
+
+    def send_first(i, p):
+        return pltpu.make_async_remote_copy(
+            src_ref=part_out.at[i, p],
+            dst_ref=first_in.at[t * n_ep + e],
+            send_sem=first_send,
+            recv_sem=first_recv,
+            device_id={"ep": p, "tp": 0},
+            device_id_type=MESH,
+        )
+
+    def start_first(i):
+        @pl.when(mine >= FAR)
+        def _():
+            each(gs, lambda p: send_first(i, p).start())
+
+        @pl.when(mine == 0)
+        def _():
+            each(n_ep - gs, lambda j: send_first(i, n_ep - 1 - j).start())
+
     def send_back(p):
         return pltpu.make_async_remote_copy(
             src_ref=back_out.at[p],
@@ -276,40 +333,84 @@
         )
 
     for i in range(n_tp):
-        dloads[i].wait()
         with jax.named_scope(f'down#i={i}'):
-            part = jnp.dot(hidden, down[i], preferred_element_type=jnp.float32)
+            part = jnp.dot(hidden[0], down[i, pl.ds(0, step)], preferred_element_type=jnp.float32)
+            for c in range(1, COLUMNS):
+                part += jnp.dot(
+                    hidden[c], down[i, pl.ds(c * step, step)], preferred_element_type=jnp.float32
+                )
             part_out[i] = part.reshape(experts, picks, sw).astype(jnp.bfloat16)
+        if i == 0:
+            @pl.when(t > 0)
+            def _():
+                start_first(0)
         if i < n_tp - 1:
             for gi in range(EARLY):
-                send_part(i, gi).start()
+                start_part(i, gi)
         if i == n_tp - 2:
             for gi in range(EARLY, GROUPS):
                 for x in range(n_tp - 1):
-                    send_part(x, gi).start()
+                    start_part(x, gi)
+
+    @pl.when(t == 0)
+    def _():
+        start_first(n_tp - 1)
+
     for gi in range(GROUPS):
         gg = group_at(gi)
-        total = part_out[n_tp - 1, pl.ds(gg * gs, gs)].astype(jnp.float32)
-        with jax.named_scope(f'rs#g={gi}'):
-            landed(part_in.at[pl.ds(0, n_tp - 1), pl.ds(gg * gs, gs)], s2_recv.at[gi])
-        for i in range(n_tp - 1):
-            total += part_in[quarter_at(i), pl.ds(gg * gs, gs)].astype(jnp.float32)
-        back_out[pl.ds(gg * gs, gs)] = total.astype(jnp.bfloat16)
-
-        def give(i):
-            p = gg * gs + i
-            if gi < GROUPS - 1:
-                send_back(p).start()
-            else:
-                @pl.when(p != e)
-                def _():
+
+        @pl.when(jnp.logical_or(t > 0, jnp.logical_not(direct(mine, gg))))
+        def _():
+            blocks = pl.ds(gg * gs, gs)
+            total = part_out[n_tp - 1, blocks].astype(jnp.float32)
+            with jax.named_scope(f'rs#g={gi}'):
+                landed(part_in.at[pl.ds(0, n_tp - 1), blocks], s2_recv.at[gi])
+            for i in range(n_tp - 1):
+                total += part_in[quarter_at(i), blocks].astype(jnp.float32)
+            back_out[blocks] = total.astype(jnp.bfloat16)
+
+            def give(i):
+                p = gg * gs + i
+                if gi < GROUPS - 1:
                     send_back(p).start()
-
-        each(gs, give)
+                else:
+                    @pl.when(p != e)
+                    def _():
+                        send_back(p).start()
+
+            each(gs, give)
+
+    near = FAR * gs
     back_in[e] = back_out[e]
-
     with jax.named_scope('backin'):
-        landed(back_in.at[pl.ds(0, n_ep - 1)], s3_recv)
+        @pl.when(t > 0)
+        def _():
+            landed(back_in.at[pl.ds(0, n_ep - 1)], s3_recv)
+
+        @pl.when(jnp.logical_and(t == 0, mine == 0))
+        def _():
+            landed(back_in.at[pl.ds(0, near - 1)], s3_recv)
+
+        @pl.when(jnp.logical_and(t == 0, mine > 0))
+        def _():
+            landed(back_in.at[pl.ds(0, n_ep - gs - 1)], s3_recv)
+
+    def take_first(low, count):
+        with jax.named_scope('firstin'):
+            landed(first_in.at[pl.ds(0, n_tp * count)], first_recv)
+        total = first_in[pl.ds(low, count)].astype(jnp.float32)
+        for i in range(1, n_tp):
+            total += first_in[pl.ds(i * n_ep + low, count)].astype(jnp.float32)
+        back_in[pl.ds(low, count)] = total.astype(jnp.bfloat16)
+
+    @pl.when(jnp.logical_and(t == 0, mine == 0))
+    def _():
+        take_first(near, n_ep - near)
+
+    @pl.when(jnp.logical_and(t == 0, mine > 0))
+    def _():
+        take_first(0, gs)
+
     with jax.named_scope("combine"):
         y = back_in[...].astype(jnp.float32).reshape(rows, sw).astype(jnp.bfloat16)
         y = jnp.concatenate([y, y, y], axis=0)
@@ -334,8 +435,23 @@
         def _():
             landed(arrived.at[pl.ds(0, n_tp - 1), pl.ds(0, gs)], fan_send)
 
-        landed(part_out.at[pl.ds(0, n_tp - 1)], s2_send)
-        landed(back_out.at[pl.ds(0, n_ep - 1)], s3_send)
+        def sent(rows_out, parts_out, backs_out):
+            if rows_out:
+                landed(first_in.at[pl.ds(0, rows_out)], first_send)
+            landed(first_in.at[pl.ds(0, parts_out)], s2_send)
+            landed(back_out.at[pl.ds(0, backs_out)], s3_send)
+
+        parts = (n_tp - 1) * n_ep
+        for low, high, rows_out in ((0, 1, n_ep - gs), (1, FAR, 0), (FAR, GROUPS, gs)):
+            here = jnp.logical_and(mine >= low, mine < high)
+
+            @pl.when(jnp.logical_and(here, t == 0))
+            def _():
+                sent(rows_out, parts, n_ep - 1 - rows_out)
+
+            @pl.when(jnp.logical_and(here, t > 0))
+            def _():
+                sent(rows_out, parts - rows_out, n_ep - 1)
 
 
 def local(tokens, chosen, chosen_weight, gate_weight, up_weight, down_weight):
@@ -367,6 +483,7 @@
             pltpu.VMEM((tok_count, 3 * experts * picks), bf),
             pltpu.VMEM((n_tp, blocks, picks, sw), bf),
             pltpu.VMEM((n_tp, blocks, picks, sw), bf),
+            pltpu.VMEM((n_tp * n_ep, picks, sw), bf),
             pltpu.VMEM((blocks, picks, sw), bf),
             pltpu.VMEM((experts, picks, sw), bf),
             dma((3,)),
@@ -382,7 +499,10 @@
             dma((GROUPS,)),
             dma,
             dma,
+            dma,
+            dma,
             pltpu.SemaphoreType.REGULAR((n_ep,)),
+            pltpu.SemaphoreType.REGULAR,
             pltpu.SemaphoreType.REGULAR,
         ],
         compiler_params=pltpu.CompilerParams(

time: 22.4 us -> 21 us (0.938)
  Pallas kernels: 21.5 us -> 20.2 us
    pallas_call x1, Pallas kernels: 21.5 us -> 20.2 us  [local(): pl.pallas_call(functools.partial(kernel, n_ep, n_tp), out_shape=jax.Shape...]
where the time goes in v2:
time: 21 us; the launch traced here: 20.9 us
  Pallas kernels  20.2 us (96%)
  local copies, waits for them, and re-layouts  0.66 us (3%)
    pallas_call x1, Pallas kernels, local(): pl.pallas_call(functools.partial(kernel, n_ep, n_tp), out_shape=jax.Shape...  20.2 us
    unnamed x1, local copies, waits for them, and re-layouts  0.66 us

profile of v2, /device:TPU:0, one launch (start us, length us, event | category | flops | bytes accessed | tf_op | source)
XLA Modules:
  0.0 20.9 jit_solution(9377404530252484601)
XLA Ops:
  0.0 20.2 %shard_map.64 = bf16[128,512]{1,0:T(8,128)(2,1)S(1)} custom-call(bf16[128,2048]{1,0:T(8,128)(2,1)} %tok_hbm.1, s32[8,8,8]{2,1,0:T(8,128)} %cho_hbm.1, f32[1,8,8]{2,1,0:T(8,128)} %wt_hbm.1, bf16[1,2048,1024]{2,1,0:T(8,128)(2,1)} %gate_hbm.1, bf16[1,2048,1024]{2,1,0:T(8,128)(2,1)} %up_hbm.1, bf16[1,1024,2048]{2,1,0:T(8,128)(2,1)} %down_hbm.1), custom_call_target="tpu_custom_call" | custom-call | tf_op jit(solution)/shard_map/pallas_call | solution.py:467
  20.2 0.7 %copy.8 = bf16[128,512]{1,0:T(8,128)(2,1)} copy(bf16[128,512]{1,0:T(8,128)(2,1)S(1)} %shard_map.64) | data formatting | bytes 262144

commit v3 on v2

--- a/solution.py
+++ b/solution.py
@@ -11,6 +11,7 @@
 GROUPS = 4
 COLUMNS = 4
 FAR = 2
+OFFSETS = (-1, 1, -2, 2)
 EARLY = 2
 
 
@@ -29,7 +30,7 @@
     tok, cho, wt, gate, up, down,
     leaving, arrived, gate_acc, up_acc, place,
     part_out, part_in, first_in, back_out, back_in,
-    in_sem, w_sem, d_sem,
+    in_sem, w_sem,
     s1_send, s1_recv, hop_send, hop_recv, fan_send, fan_recv, s2_send, s2_recv, s3_send, s3_recv, first_send, first_recv,
     ep_ready, tp_seen, tp_ready,
 ):
@@ -51,10 +52,16 @@
         up = jnp.where(i < mine, i, i + 1)
         return jnp.where(mine == 0, top, jnp.where(mine < GROUPS // 2, down, up))
 
-    def direct(src, dst):
-        return jnp.logical_or(
-            jnp.logical_and(dst == 0, src >= FAR), jnp.logical_and(src == 0, dst > 0)
-        )
+    def is_first(i):
+        if i == 0:
+            return t > 0
+        return t == 0 if i == n_tp - 1 else t < 0
+
+    def direct(i, src, dst):
+        near = jnp.logical_or(dst == 0, src == 0)
+        near = jnp.logical_and(near, dst != src)
+        far = jnp.logical_and(dst == 0, src >= FAR)
+        return jnp.where(is_first(i), near, far)
 
     def quarter_at(i):
         if i == n_tp - 1:
@@ -85,17 +92,14 @@
     for c in loads:
         c.start()
     wloads = []
-    for k in range(n_tp):
-        piece = pl.ds(k * sw, sw)
-        a = pltpu.make_async_copy(gate_hbm.at[0, piece, :], gate.at[piece, :], w_sem.at[0, k])
-        b = pltpu.make_async_copy(up_hbm.at[0, piece, :], up.at[piece, :], w_sem.at[1, k])
-        wloads.append((a, b))
-    dloads = []
     for i in range(n_tp):
+        deep = pl.ds(i * sw, sw)
         col = pl.multiple_of(quarter_at(i) * sw, sw)
-        dloads.append(
-            pltpu.make_async_copy(down_hbm.at[0, :, pl.ds(col, sw)], down.at[i], d_sem.at[i])
-        )
+        wloads += [
+            pltpu.make_async_copy(gate_hbm.at[0, deep, :], gate.at[deep, :], w_sem),
+            pltpu.make_async_copy(up_hbm.at[0, deep, :], up.at[deep, :], w_sem),
+            pltpu.make_async_copy(down_hbm.at[0, :, pl.ds(col, sw)], down.at[i], w_sem),
+        ]
 
     with jax.named_scope("barrier"):
         floor = e + jnp.minimum(t, 1)
@@ -117,10 +121,7 @@
     with jax.named_scope("loadwait"):
         for c in loads:
             c.wait()
-    for a, b in wloads:
-        a.start()
-        b.start()
-    for c in dloads:
+    for c in wloads:
         c.start()
 
     lane = lax.broadcasted_iota(jnp.int32, (picks, picks), 1)
@@ -151,16 +152,26 @@
             device_id_type=MESH,
         )
 
-    def send_hop(p):
+    def send_hop(slot, p):
         return pltpu.make_async_remote_copy(
             src_ref=leaving.at[t, p],
             dst_ref=arrived.at[t, e],
             send_sem=hop_send,
-            recv_sem=hop_recv,
+            recv_sem=hop_recv.at[slot],
             device_id={"ep": p},
             device_id_type=MESH,
         )
 
+    def hop_group(slot, g):
+        each(gs, lambda i: send_hop(slot, g * gs + i).start())
+
+    def hop_odd(slot, g):
+        each(gs // 2, lambda i: send_hop(slot, g * gs + 2 * i + 1).start())
+
+    def send_even(g):
+        for k in range(n_tp):
+            each(gs // 2, lambda i: send_tokens(k, g * gs + 2 * i).start())
+
     def send_group(g):
         for k in range(n_tp):
             each(gs, lambda i: send_tokens(k, g * gs + i).start())
@@ -169,7 +180,20 @@
         each(gs, lambda i: pl.semaphore_wait(ep_ready.at[g * gs + i], 1))
 
     with jax.named_scope("senddown"):
-        pl.loop(0, mine)(send_group)
+        @pl.when(mine > 0)
+        def _():
+            hop_group(1, mine - 1)
+
+        @pl.when(mine > 1)
+        def _():
+            hop_odd(3, mine - 2)
+
+        pl.loop(0, mine - 2)(send_group)
+
+        @pl.when(mine > 1)
+        def _():
+            send_even(mine - 2)
+
 
         def send_near(i):
             p = mine * gs + i
@@ -188,7 +212,7 @@
         @pl.when(mine < GROUPS - 1)
         def _():
             ready_group(mine + 1)
-            each(gs, lambda i: send_hop((mine + 1) * gs + i).start())
+            hop_group(0, mine + 1)
 
     with jax.named_scope("tpseen"):
         @pl.when(t == 0)
@@ -205,7 +229,13 @@
             ready_group(g)
             send_group(g)
 
-        pl.loop(mine + 2, GROUPS)(send_up)
+        @pl.when(mine == 0)
+        def _():
+            ready_group(2)
+            hop_odd(2, 2)
+            send_even(2)
+
+        pl.loop(jnp.maximum(mine + 2, 3), GROUPS)(send_up)
 
     parts = []
     for x in range(experts):
@@ -226,12 +256,23 @@
     def _():
         pl.semaphore_wait(tp_ready, 1)
 
-    below = pl.ds((mine - 1) * gs, gs)
-
-    def send_fan(i):
+    odd = lax.rem(e, 2)
+    both = jnp.logical_and(mine > 0, mine < GROUPS - 1)
+
+    def split_from(slot):
+        src = mine + OFFSETS[slot]
+        near = jnp.logical_and(src >= 0, src < GROUPS)
+        if slot < 2:
+            return near
+        if slot == 2:
+            near = src == 0
+        return jnp.logical_and(near, odd == 1)
+
+    def send_fan(slot, i):
+        blocks = pl.ds((mine + OFFSETS[slot]) * gs, gs)
         return pltpu.make_async_remote_copy(
-            src_ref=arrived.at[t, below],
-            dst_ref=arrived.at[t, below],
+            src_ref=arrived.at[t, blocks],
+            dst_ref=arrived.at[t, blocks],
             send_sem=fan_send,
             recv_sem=fan_recv.at[t],
             device_id={"tp": quarter_at(i)},
@@ -239,35 +280,37 @@
         )
 
     with jax.named_scope("fan"):
-        @pl.when(mine > 0)
-        def _():
-            landed(arrived.at[t, pl.ds(0, gs)], hop_recv)
-            for i in range(n_tp - 1):
-                send_fan(i).start()
+        for slot in range(4):
+            @pl.when(split_from(slot))
+            def _():
+                landed(arrived.at[t, pl.ds(0, gs)], hop_recv.at[slot])
+                for i in range(n_tp - 1):
+                    send_fan(slot, i).start()
 
     for k in range(n_tp):
         arrived[k, e] = leaving[k, e]
-    for a, b in wloads:
-        a.wait()
-        b.wait()
-    for c in dloads:
-        c.wait()
+    landed(gate, w_sem)
+    landed(up, w_sem)
+    landed(down, w_sem)
     hid = gate.shape[1]
     step = hid // COLUMNS
     hidden = []
     for k in range(n_tp):
         with jax.named_scope(f'tokin#k={k}'):
-            @pl.when(mine == 0)
-            def _():
-                landed(arrived.at[k, pl.ds(0, n_ep - 1)], s1_recv.at[k])
-
-            @pl.when(mine > 0)
-            def _():
-                landed(arrived.at[k, pl.ds(0, n_ep - 1 - gs)], s1_recv.at[k])
-
-            @pl.when(jnp.logical_and(mine > 0, t != k))
-            def _():
-                landed(arrived.at[k, pl.ds(0, gs)], fan_recv.at[k])
+            for sides in (1, 2):
+                for parity in (0, 1):
+                    here = both if sides == 2 else jnp.logical_not(both)
+                    more = jnp.logical_and(odd == 1, mine < GROUPS - 1)
+                    here = jnp.logical_and(here, more == (parity == 1))
+
+                    @pl.when(here)
+                    def _():
+                        split = gs * (sides + parity)
+                        landed(arrived.at[k, pl.ds(0, n_ep - 1 - split)], s1_recv.at[k])
+
+                        @pl.when(t != k)
+                        def _():
+                            landed(arrived.at[k, pl.ds(0, split)], fan_recv.at[k])
 
         x = arrived[k].astype(jnp.float32).reshape(rows, sw).astype(jnp.bfloat16)
         deep = pl.ds(k * sw, sw)
@@ -296,12 +339,9 @@
         )
 
     def start_part(i, gi):
-        if i > 0:
+        @pl.when(jnp.logical_not(direct(i, mine, group_at(gi))))
+        def _():
             send_part(i, gi).start()
-        else:
-            @pl.when(jnp.logical_or(t == 0, jnp.logical_not(direct(mine, group_at(gi)))))
-            def _():
-                send_part(i, gi).start()
 
     def send_first(i, p):
         return pltpu.make_async_remote_copy(
@@ -309,16 +349,16 @@
             dst_ref=first_in.at[t * n_ep + e],
             send_sem=first_send,
             recv_sem=first_recv,
-            device_id={"ep": p, "tp": 0},
+            device_id={"ep": p, "tp": quarter_at(i)},
             device_id_type=MESH,
         )
 
     def start_first(i):
-        @pl.when(mine >= FAR)
+        @pl.when(jnp.logical_and(direct(i, mine, 0), mine > 0))
         def _():
             each(gs, lambda p: send_first(i, p).start())
 
-        @pl.when(mine == 0)
+        @pl.when(jnp.logical_and(is_first(i), mine == 0))
         def _():
             each(n_ep - gs, lambda j: send_first(i, n_ep - 1 - j).start())
 
@@ -341,25 +381,27 @@
                 )
             part_out[i] = part.reshape(experts, picks, sw).astype(jnp.bfloat16)
         if i == 0:
-            @pl.when(t > 0)
-            def _():
-                start_first(0)
+            @pl.when(jnp.logical_and(t > 0, mine == 0))
+            def _():
+                send_part(0, GROUPS - 1).start()
+        start_first(i)
         if i < n_tp - 1:
             for gi in range(EARLY):
                 start_part(i, gi)
         if i == n_tp - 2:
             for gi in range(EARLY, GROUPS):
                 for x in range(n_tp - 1):
-                    start_part(x, gi)
-
-    @pl.when(t == 0)
-    def _():
-        start_first(n_tp - 1)
+                    if x or gi < GROUPS - 1:
+                        start_part(x, gi)
+                    else:
+                        @pl.when(jnp.logical_or(t == 0, mine > 0))
+                        def _():
+                            start_part(x, gi)
 
     for gi in range(GROUPS):
         gg = group_at(gi)
 
-        @pl.when(jnp.logical_or(t > 0, jnp.logical_not(direct(mine, gg))))
+        @pl.when(jnp.logical_not(direct(n_tp - 1, mine, gg)))
         def _():
             blocks = pl.ds(gg * gs, gs)
             total = part_out[n_tp - 1, blocks].astype(jnp.float32)
@@ -380,20 +422,7 @@
 
             each(gs, give)
 
-    near = FAR * gs
     back_in[e] = back_out[e]
-    with jax.named_scope('backin'):
-        @pl.when(t > 0)
-        def _():
-            landed(back_in.at[pl.ds(0, n_ep - 1)], s3_recv)
-
-        @pl.when(jnp.logical_and(t == 0, mine == 0))
-        def _():
-            landed(back_in.at[pl.ds(0, near - 1)], s3_recv)
-
-        @pl.when(jnp.logical_and(t == 0, mine > 0))
-        def _():
-            landed(back_in.at[pl.ds(0, n_ep - gs - 1)], s3_recv)
 
     def take_first(low, count):
         with jax.named_scope('firstin'):
@@ -403,13 +432,18 @@
             total += first_in[pl.ds(i * n_ep + low, count)].astype(jnp.float32)
         back_in[pl.ds(low, count)] = total.astype(jnp.bfloat16)
 
-    @pl.when(jnp.logical_and(t == 0, mine == 0))
-    def _():
-        take_first(near, n_ep - near)
-
-    @pl.when(jnp.logical_and(t == 0, mine > 0))
-    def _():
-        take_first(0, gs)
+    for here, low, count in (
+        (jnp.logical_and(t == 0, mine == 0), gs, n_ep - gs),
+        (jnp.logical_and(t == 0, mine > 0), 0, gs),
+        (jnp.logical_and(t > 0, mine == 0), FAR * gs, n_ep - FAR * gs),
+        (jnp.logical_and(t > 0, mine > 0), 0, 0),
+    ):
+        @pl.when(here)
+        def _():
+            with jax.named_scope('backin'):
+                landed(back_in.at[pl.ds(0, n_ep - 1 - count)], s3_recv)
+            if count:
+                take_first(low, count)
 
     with jax.named_scope("combine"):
         y = back_in[...].astype(jnp.float32).reshape(rows, sw).astype(jnp.bfloat16)
@@ -418,40 +452,48 @@
         out_ref[...] = result.astype(out_ref.dtype)
 
     with jax.named_scope("drain"):
-        for k in range(n_tp):
-            @pl.when(mine == GROUPS - 1)
-            def _():
-                landed(leaving.at[k, pl.ds(0, n_ep - 1)], s1_send)
-
-            @pl.when(mine < GROUPS - 1)
-            def _():
-                landed(leaving.at[k, pl.ds(0, n_ep - 1 - gs)], s1_send)
-
-        @pl.when(mine < GROUPS - 1)
-        def _():
-            landed(leaving.at[0, pl.ds(0, gs)], hop_send)
-
-        @pl.when(mine > 0)
-        def _():
-            landed(arrived.at[pl.ds(0, n_tp - 1), pl.ds(0, gs)], fan_send)
-
-        def sent(rows_out, parts_out, backs_out):
-            if rows_out:
-                landed(first_in.at[pl.ds(0, rows_out)], first_send)
-            landed(first_in.at[pl.ds(0, parts_out)], s2_send)
-            landed(back_out.at[pl.ds(0, backs_out)], s3_send)
-
-        parts = (n_tp - 1) * n_ep
-        for low, high, rows_out in ((0, 1, n_ep - gs), (1, FAR, 0), (FAR, GROUPS, gs)):
+        def sent_tokens(hops):
+            for k in range(n_tp):
+                landed(leaving.at[k, pl.ds(0, n_ep - 1 - hops)], s1_send)
+            landed(leaving.at[0, pl.ds(0, hops)], hop_send)
+
+        @pl.when(jnp.logical_not(both))
+        def _():
+            sent_tokens(gs + gs // 2)
+
+        @pl.when(mine == 1)
+        def _():
+            sent_tokens(2 * gs)
+
+        @pl.when(jnp.logical_and(both, mine > 1))
+        def _():
+            sent_tokens(2 * gs + gs // 2)
+
+        for slot in range(4):
+            @pl.when(split_from(slot))
+            def _():
+                landed(arrived.at[pl.ds(0, n_tp - 1), pl.ds(0, gs)], fan_send)
+
+        def sent(firsts, parts, backs):
+            if firsts:
+                landed(first_in.at[pl.ds(0, firsts)], first_send)
+            landed(first_in.at[pl.ds(0, parts)], s2_send)
+            landed(back_out.at[pl.ds(0, backs)], s3_send)
+
+        for low, high in ((0, 1), (1, FAR), (FAR, GROUPS)):
             here = jnp.logical_and(mine >= low, mine < high)
+            lead = gs if low else n_ep - gs
+            rest = gs if low == FAR else 0
+            firsts = lead + (n_tp - 1) * rest
 
             @pl.when(jnp.logical_and(here, t == 0))
             def _():
-                sent(rows_out, parts, n_ep - 1 - rows_out)
+                sent(firsts, (n_tp - 1) * (n_ep - rest), n_ep - 1 - lead)
 
             @pl.when(jnp.logical_and(here, t > 0))
             def _():
-                sent(rows_out, parts - rows_out, n_ep - 1)
+                parts = n_ep - lead + (n_tp - 2) * (n_ep - rest)
+                sent(firsts, parts, n_ep - 1 - rest)
 
 
 def local(tokens, chosen, chosen_weight, gate_weight, up_weight, down_weight):
@@ -487,12 +529,11 @@
             pltpu.VMEM((blocks, picks, sw), bf),
             pltpu.VMEM((experts, picks, sw), bf),
             dma((3,)),
-            dma((2, n_tp)),
+            dma,
+            dma,
             dma((n_tp,)),
             dma,
-            dma((n_tp,)),
-            dma,
-            dma,
+            dma((4,)),
             dma,
             dma((n_tp,)),
             dma,

time: 21 us -> 19.5 us (0.929)
  the two profiles are of different devices: /device:TPU:0 before, /device:TPU:9 now
where the time goes in v3:
time: 19.5 us; the launch traced here: 19.3 us
  Pallas kernels  18.7 us (96%)
  local copies, waits for them, and re-layouts  0.66 us (3%)
    pallas_call x1, Pallas kernels, local(): pl.pallas_call(functools.partial(kernel, n_ep, n_tp), out_shape=jax.Shape...  18.7 us
    unnamed x1, local copies, waits for them, and re-layouts  0.66 us

profile of v3, /device:TPU:9, one launch (start us, length us, event | category | flops | bytes accessed | tf_op | source)
XLA Modules:
  0.0 19.3 jit_solution(14602064870718881807)
XLA Ops:
  0.0 18.7 %shard_map.64 = bf16[128,512]{1,0:T(8,128)(2,1)S(1)} custom-call(bf16[128,2048]{1,0:T(8,128)(2,1)} %tok_hbm.1, s32[8,8,8]{2,1,0:T(8,128)} %cho_hbm.1, f32[1,8,8]{2,1,0:T(8,128)} %wt_hbm.1, bf16[1,2048,1024]{2,1,0:T(8,128)(2,1)} %gate_hbm.1, bf16[1,2048,1024]{2,1,0:T(8,128)(2,1)} %up_hbm.1, bf16[1,1024,2048]{2,1,0:T(8,128)(2,1)} %down_hbm.1), custom_call_target="tpu_custom_call" | custom-call | tf_op jit(solution)/shard_map/pallas_call | solution.py:509
  18.7 0.7 %copy.8 = bf16[128,512]{1,0:T(8,128)(2,1)} copy(bf16[128,512]{1,0:T(8,128)(2,1)S(1)} %shard_map.64) | data formatting | bytes 262144

commit v4 on v3

--- a/solution.py
+++ b/solution.py
@@ -10,8 +10,9 @@
 MESH = pl.DeviceIdType.MESH
 GROUPS = 4
 COLUMNS = 4
-FAR = 2
-OFFSETS = (-1, 1, -2, 2)
+FIRST = ((1, 0), (2, 0), (3, 0), (0, 1), (0, 2), (0, 3))
+EVERY = ((2, 0), (3, 0), (3, 1), (0, 2), (0, 3))
+SPLIT = (((1, 2), (2, 1)), ((1, 2), (2, 1), (0, 2), (2, 0)))
 EARLY = 2
 
 
@@ -31,8 +32,8 @@
     leaving, arrived, gate_acc, up_acc, place,
     part_out, part_in, first_in, back_out, back_in,
     in_sem, w_sem,
-    s1_send, s1_recv, hop_send, hop_recv, fan_send, fan_recv, s2_send, s2_recv, s3_send, s3_recv, first_send, first_recv,
-    ep_ready, tp_seen, tp_ready,
+    s1_send, s1_recv, hop_send, hop_recv, fan_send, s2_send, s2_recv, s3_send, s3_recv, first_send, first_recv,
+    ep_ready, tp_seen, tp_ready, tp_above,
 ):
     e = lax.axis_index("ep")
     t = lax.axis_index("tp")
@@ -52,23 +53,31 @@
         up = jnp.where(i < mine, i, i + 1)
         return jnp.where(mine == 0, top, jnp.where(mine < GROUPS // 2, down, up))
 
-    def is_first(i):
+    def any_of(terms):
+        out = mine < 0
+        for term in terms:
+            out = jnp.logical_or(out, term)
+        return out
+
+    def direct(i, dst):
+        pairs = EVERY if i else FIRST
+        return any_of(jnp.logical_and(mine == a, dst == b) for a, b in pairs)
+
+    def quarter_at(i):
+        if i == 0:
+            return 0
+        others = t if i == n_tp - 1 else jnp.where(i < t, i, i + 1)
+        return jnp.where(t == 0, n_tp - i, others)
+
+    def leaves(i):
         if i == 0:
             return t > 0
-        return t == 0 if i == n_tp - 1 else t < 0
-
-    def direct(i, src, dst):
-        near = jnp.logical_or(dst == 0, src == 0)
-        near = jnp.logical_and(near, dst != src)
-        far = jnp.logical_and(dst == 0, src >= FAR)
-        return jnp.where(is_first(i), near, far)
-
-    def quarter_at(i):
-        if i == n_tp - 1:
-            return t
-        down_first = n_tp - 1 - i
-        up_first = jnp.where(i < t, i, i + 1)
-        return jnp.where(t == 0, down_first, up_first)
+        return t == 0 if i == n_tp - 1 else t >= 0
+
+    own_at = jnp.where(t == 0, 0, n_tp - 1)
+
+    def slice_at(i):
+        return lax.rem(t + i, n_tp)
 
     barrier = pltpu.get_barrier_semaphore()
 
@@ -93,7 +102,7 @@
         c.start()
     wloads = []
     for i in range(n_tp):
-        deep = pl.ds(i * sw, sw)
+        deep = pl.ds(pl.multiple_of(slice_at(i) * sw, sw), sw)
         col = pl.multiple_of(quarter_at(i) * sw, sw)
         wloads += [
             pltpu.make_async_copy(gate_hbm.at[0, deep, :], gate.at[deep, :], w_sem),
@@ -162,57 +171,73 @@
             device_id_type=MESH,
         )
 
-    def hop_group(slot, g):
-        each(gs, lambda i: send_hop(slot, g * gs + i).start())
-
-    def hop_odd(slot, g):
-        each(gs // 2, lambda i: send_hop(slot, g * gs + 2 * i + 1).start())
-
-    def send_even(g):
-        for k in range(n_tp):
-            each(gs // 2, lambda i: send_tokens(k, g * gs + 2 * i).start())
-
-    def send_group(g):
-        for k in range(n_tp):
-            each(gs, lambda i: send_tokens(k, g * gs + i).start())
+    odd = lax.rem(e, 2)
+
+    def split_to(parity, dst):
+        return any_of([mine == a for a, b in SPLIT[parity] if b == dst])
+
+    def split_from(src):
+        return any_of(
+            jnp.logical_and(mine == b, odd == parity)
+            for parity in range(2)
+            for a, b in SPLIT[parity]
+            if a == src
+        )
+
+    def hops_to(dst):
+        for parity in range(2):
+            for a, b in SPLIT[parity]:
+                if b == dst:
+                    @pl.when(mine == a)
+                    def _():
+                        each(gs // 2, lambda i: send_hop(a, b * gs + 2 * i + parity).start())
+
+    def direct_to(dst):
+        @pl.when(jnp.logical_not(split_to(1, dst)))
+        def _():
+            for i in range(n_tp):
+                k = slice_at(i)
+                each(gs, lambda j: send_tokens(k, dst * gs + j).start())
+
+        @pl.when(jnp.logical_and(split_to(1, dst), jnp.logical_not(split_to(0, dst))))
+        def _():
+            for i in range(n_tp):
+                k = slice_at(i)
+                each(gs // 2, lambda j: send_tokens(k, dst * gs + 2 * j).start())
 
     def ready_group(g):
         each(gs, lambda i: pl.semaphore_wait(ep_ready.at[g * gs + i], 1))
 
     with jax.named_scope("senddown"):
-        @pl.when(mine > 0)
-        def _():
-            hop_group(1, mine - 1)
-
-        @pl.when(mine > 1)
-        def _():
-            hop_odd(3, mine - 2)
-
-        pl.loop(0, mine - 2)(send_group)
-
-        @pl.when(mine > 1)
-        def _():
-            send_even(mine - 2)
-
+        for dst in range(GROUPS - 2, -1, -1):
+            @pl.when(mine > dst)
+            def _():
+                hops_to(dst)
+
+        for dst in range(GROUPS - 1):
+            @pl.when(mine > dst)
+            def _():
+                direct_to(dst)
 
         def send_near(i):
             p = mine * gs + i
+            p = jnp.where(p < e, p, p + 1)
 
             @pl.when(p > e)
             def _():
                 pl.semaphore_wait(ep_ready.at[p], 1)
 
-            @pl.when(p != e)
-            def _():
-                for k in range(n_tp):
-                    send_tokens(k, p).start()
-
-        each(gs, send_near)
+            for k in range(n_tp):
+                send_tokens(k, p).start()
+
+        each(gs - 1, send_near)
     with jax.named_scope("hop"):
-        @pl.when(mine < GROUPS - 1)
-        def _():
-            ready_group(mine + 1)
-            hop_group(0, mine + 1)
+        for dst in range(1, GROUPS):
+            @pl.when(mine == dst - 1)
+            def _():
+                ready_group(dst)
+                hops_to(dst)
+                direct_to(dst)
 
     with jax.named_scope("tpseen"):
         @pl.when(t == 0)
@@ -225,17 +250,12 @@
             pl.loop(1, n_tp)(admit)
 
     with jax.named_scope("sendup"):
-        def send_up(g):
-            ready_group(g)
-            send_group(g)
-
-        @pl.when(mine == 0)
-        def _():
-            ready_group(2)
-            hop_odd(2, 2)
-            send_even(2)
-
-        pl.loop(jnp.maximum(mine + 2, 3), GROUPS)(send_up)
+        for dst in range(2, GROUPS):
+            @pl.when(mine < dst - 1)
+            def _():
+                ready_group(dst)
+                hops_to(dst)
+                direct_to(dst)
 
     parts = []
     for x in range(experts):
@@ -256,72 +276,72 @@
     def _():
         pl.semaphore_wait(tp_ready, 1)
 
-    odd = lax.rem(e, 2)
-    both = jnp.logical_and(mine > 0, mine < GROUPS - 1)
-
-    def split_from(slot):
-        src = mine + OFFSETS[slot]
-        near = jnp.logical_and(src >= 0, src < GROUPS)
-        if slot < 2:
-            return near
-        if slot == 2:
-            near = src == 0
-        return jnp.logical_and(near, odd == 1)
+    @pl.when(mine == 0)
+    def _():
+        for i in range(n_tp - 1):
+            pl.semaphore_signal(
+                tp_above, inc=1, device_id={"tp": lax.rem(t + 1 + i, n_tp)}, device_id_type=MESH
+            )
 
     def send_fan(slot, i):
-        blocks = pl.ds((mine + OFFSETS[slot]) * gs, gs)
+        blocks = pl.ds(slot * gs, gs)
         return pltpu.make_async_remote_copy(
             src_ref=arrived.at[t, blocks],
             dst_ref=arrived.at[t, blocks],
             send_sem=fan_send,
-            recv_sem=fan_recv.at[t],
-            device_id={"tp": quarter_at(i)},
+            recv_sem=s1_recv.at[t],
+            device_id={"tp": lax.rem(t + 1 + i, n_tp)},
             device_id_type=MESH,
         )
 
     with jax.named_scope("fan"):
-        for slot in range(4):
+        for slot in range(GROUPS):
             @pl.when(split_from(slot))
             def _():
                 landed(arrived.at[t, pl.ds(0, gs)], hop_recv.at[slot])
                 for i in range(n_tp - 1):
                     send_fan(slot, i).start()
 
+    heard = {}
+    for group in range(GROUPS):
+        for parity in range(2):
+            count = gs * sum(b == group for _, b in SPLIT[parity])
+            case = jnp.logical_and(mine == group, odd == parity)
+            heard[count] = jnp.logical_or(heard[count], case) if count in heard else case
+
     for k in range(n_tp):
         arrived[k, e] = leaving[k, e]
+    @pl.when(mine == 0)
+    def _():
+        pl.semaphore_wait(tp_above, n_tp - 1)
+
     landed(gate, w_sem)
     landed(up, w_sem)
     landed(down, w_sem)
     hid = gate.shape[1]
     step = hid // COLUMNS
     hidden = []
-    for k in range(n_tp):
-        with jax.named_scope(f'tokin#k={k}'):
-            for sides in (1, 2):
-                for parity in (0, 1):
-                    here = both if sides == 2 else jnp.logical_not(both)
-                    more = jnp.logical_and(odd == 1, mine < GROUPS - 1)
-                    here = jnp.logical_and(here, more == (parity == 1))
-
-                    @pl.when(here)
+    for i in range(n_tp):
+        k = slice_at(i)
+        with jax.named_scope(f'tokin#k={i}'):
+            if i:
+                landed(arrived.at[k, pl.ds(0, n_ep - 1)], s1_recv.at[k])
+            else:
+                for count in sorted(heard):
+                    @pl.when(heard[count])
                     def _():
-                        split = gs * (sides + parity)
-                        landed(arrived.at[k, pl.ds(0, n_ep - 1 - split)], s1_recv.at[k])
-
-                        @pl.when(t != k)
-                        def _():
-                            landed(arrived.at[k, pl.ds(0, split)], fan_recv.at[k])
+                        landed(arrived.at[k, pl.ds(0, n_ep - 1 - count)], s1_recv.at[k])
 
         x = arrived[k].astype(jnp.float32).reshape(rows, sw).astype(jnp.bfloat16)
-        deep = pl.ds(k * sw, sw)
+        deep = pl.ds(pl.multiple_of(k * sw, sw), sw)
         for c in range(COLUMNS):
             cols = pl.ds(c * step, step)
             g = jnp.dot(x, gate[deep, cols], preferred_element_type=jnp.float32)
             u = jnp.dot(x, up[deep, cols], preferred_element_type=jnp.float32)
-            if k > 0:
+            if i > 0:
                 g += gate_acc[:, cols]
                 u += up_acc[:, cols]
-            if k < n_tp - 1:
+            if i < n_tp - 1:
                 gate_acc[:, cols] = g
                 up_acc[:, cols] = u
             else:
@@ -338,8 +358,8 @@
             device_id_type=MESH,
         )
 
-    def start_part(i, gi):
-        @pl.when(jnp.logical_not(direct(i, mine, group_at(gi))))
+    def start_part(i, gi, when):
+        @pl.when(jnp.logical_and(when, jnp.logical_not(direct(i, group_at(gi)))))
         def _():
             send_part(i, gi).start()
 
@@ -354,13 +374,10 @@
         )
 
     def start_first(i):
-        @pl.when(jnp.logical_and(direct(i, mine, 0), mine > 0))
-        def _():
-            each(gs, lambda p: send_first(i, p).start())
-
-        @pl.when(jnp.logical_and(is_first(i), mine == 0))
-        def _():
-            each(n_ep - gs, lambda j: send_first(i, n_ep - 1 - j).start())
+        for dst in (0, *range(GROUPS - 1, 0, -1)):
+            @pl.when(direct(i, dst))
+            def _():
+                each(gs, lambda j: send_first(i, dst * gs + j).start())
 
     def send_back(p):
         return pltpu.make_async_remote_copy(
@@ -381,34 +398,36 @@
                 )
             part_out[i] = part.reshape(experts, picks, sw).astype(jnp.bfloat16)
         if i == 0:
-            @pl.when(jnp.logical_and(t > 0, mine == 0))
-            def _():
-                send_part(0, GROUPS - 1).start()
+            start_part(0, GROUPS - 1, jnp.logical_and(t > 0, mine == 0))
         start_first(i)
+        here = leaves(i)
         if i < n_tp - 1:
             for gi in range(EARLY):
-                start_part(i, gi)
+                start_part(i, gi, here)
+            for gi in range(EARLY, GROUPS - 1):
+                start_part(i, gi, jnp.logical_and(here, mine != 1))
+        else:
+            for gi in range(GROUPS):
+                start_part(i, gi, here)
         if i == n_tp - 2:
             for gi in range(EARLY, GROUPS):
                 for x in range(n_tp - 1):
-                    if x or gi < GROUPS - 1:
-                        start_part(x, gi)
-                    else:
-                        @pl.when(jnp.logical_or(t == 0, mine > 0))
-                        def _():
-                            start_part(x, gi)
+                    late = mine == 1 if gi < GROUPS - 1 else mine > (0 if x == 0 else -1)
+                    start_part(x, gi, jnp.logical_and(leaves(x), late))
 
     for gi in range(GROUPS):
         gg = group_at(gi)
 
-        @pl.when(jnp.logical_not(direct(n_tp - 1, mine, gg)))
+        ended = jnp.where(t == 0, direct(0, gg), direct(1, gg))
+
+        @pl.when(jnp.logical_not(ended))
         def _():
             blocks = pl.ds(gg * gs, gs)
-            total = part_out[n_tp - 1, blocks].astype(jnp.float32)
+            total = part_out[own_at, blocks].astype(jnp.float32)
             with jax.named_scope(f'rs#g={gi}'):
                 landed(part_in.at[pl.ds(0, n_tp - 1), blocks], s2_recv.at[gi])
             for i in range(n_tp - 1):
-                total += part_in[quarter_at(i), blocks].astype(jnp.float32)
+                total += part_in[lax.rem(t + 1 + i, n_tp), blocks].astype(jnp.float32)
             back_out[blocks] = total.astype(jnp.bfloat16)
 
             def give(i):
@@ -423,77 +442,69 @@
             each(gs, give)
 
     back_in[e] = back_out[e]
-
-    def take_first(low, count):
-        with jax.named_scope('firstin'):
-            landed(first_in.at[pl.ds(0, n_tp * count)], first_recv)
-        total = first_in[pl.ds(low, count)].astype(jnp.float32)
-        for i in range(1, n_tp):
-            total += first_in[pl.ds(i * n_ep + low, count)].astype(jnp.float32)
-        back_in[pl.ds(low, count)] = total.astype(jnp.bfloat16)
-
-    for here, low, count in (
-        (jnp.logical_and(t == 0, mine == 0), gs, n_ep - gs),
-        (jnp.logical_and(t == 0, mine > 0), 0, gs),
-        (jnp.logical_and(t > 0, mine == 0), FAR * gs, n_ep - FAR * gs),
-        (jnp.logical_and(t > 0, mine > 0), 0, 0),
-    ):
-        @pl.when(here)
+    with jax.named_scope("drain"):
+        for group in range(GROUPS):
+            @pl.when(mine == group)
+            def _():
+                hops = gs // 2 * sum(a == group for pairs in SPLIT for a, _ in pairs)
+                for k in range(n_tp):
+                    landed(leaving.at[k, pl.ds(0, n_ep - 1 - hops)], s1_send)
+                if hops:
+                    landed(leaving.at[0, pl.ds(0, hops)], hop_send)
+
+        for slot in range(GROUPS):
+            @pl.when(split_from(slot))
+            def _():
+                landed(arrived.at[pl.ds(0, n_tp - 1), pl.ds(0, gs)], fan_send)
+
+        def sent(lead, rest):
+            firsts = gs * (lead + (n_tp - 1) * rest)
+            if firsts:
+                landed(first_in.at[pl.ds(0, firsts)], first_send)
+
+            @pl.when(t == 0)
+            def _():
+                parts = (n_tp - 1) * (n_ep - gs * rest)
+                landed(first_in.at[pl.ds(0, parts)], s2_send)
+                landed(back_out.at[pl.ds(0, n_ep - 1 - gs * lead)], s3_send)
+
+            @pl.when(t > 0)
+            def _():
+                parts = n_ep - gs * lead + (n_tp - 2) * (n_ep - gs * rest)
+                landed(first_in.at[pl.ds(0, parts)], s2_send)
+                landed(back_out.at[pl.ds(0, n_ep - 1 - gs * rest)], s3_send)
+
+        for group in range(GROUPS):
+            @pl.when(mine == group)
+            def _():
+                sent(sum(a == group for a, _ in FIRST), sum(a == group for a, _ in EVERY))
+
+    ends = {}
+    for group in range(GROUPS):
+        for pairs, here in ((FIRST, t == 0), (EVERY, t > 0)):
+            case = jnp.logical_and(mine == group, here)
+            come = tuple(sorted(a for a, b in pairs if b == group))
+            ends[come] = jnp.logical_or(ends[come], case) if come in ends else case
+
+    for come in sorted(ends):
+        @pl.when(ends[come])
         def _():
             with jax.named_scope('backin'):
-                landed(back_in.at[pl.ds(0, n_ep - 1 - count)], s3_recv)
-            if count:
-                take_first(low, count)
+                landed(back_in.at[pl.ds(0, n_ep - 1 - gs * len(come))], s3_recv)
+            if come:
+                with jax.named_scope('firstin'):
+                    landed(first_in.at[pl.ds(0, n_tp * gs * len(come))], first_recv)
+            for src in come:
+                total = first_in[pl.ds(src * gs, gs)].astype(jnp.float32)
+                for i in range(1, n_tp):
+                    total += first_in[pl.ds(i * n_ep + src * gs, gs)].astype(jnp.float32)
+                back_in[pl.ds(src * gs, gs)] = total.astype(jnp.bfloat16)
 
     with jax.named_scope("combine"):
         y = back_in[...].astype(jnp.float32).reshape(rows, sw).astype(jnp.bfloat16)
         y = jnp.concatenate([y, y, y], axis=0)
         result = jnp.dot(place[...], y, preferred_element_type=jnp.float32)
         out_ref[...] = result.astype(out_ref.dtype)
-
-    with jax.named_scope("drain"):
-        def sent_tokens(hops):
-            for k in range(n_tp):
-                landed(leaving.at[k, pl.ds(0, n_ep - 1 - hops)], s1_send)
-            landed(leaving.at[0, pl.ds(0, hops)], hop_send)
-
-        @pl.when(jnp.logical_not(both))
-        def _():
-            sent_tokens(gs + gs // 2)
-
-        @pl.when(mine == 1)
-        def _():
-            sent_tokens(2 * gs)
-
-        @pl.when(jnp.logical_and(both, mine > 1))
-        def _():
-            sent_tokens(2 * gs + gs // 2)
-
-        for slot in range(4):
-            @pl.when(split_from(slot))
-            def _():
-                landed(arrived.at[pl.ds(0, n_tp - 1), pl.ds(0, gs)], fan_send)
-
-        def sent(firsts, parts, backs):
-            if firsts:
-                landed(first_in.at[pl.ds(0, firsts)], first_send)
-            landed(first_in.at[pl.ds(0, parts)], s2_send)
-            landed(back_out.at[pl.ds(0, backs)], s3_send)
-
-        for low, high in ((0, 1), (1, FAR), (FAR, GROUPS)):
-            here = jnp.logical_and(mine >= low, mine < high)
-            lead = gs if low else n_ep - gs
-            rest = gs if low == FAR else 0
-            firsts = lead + (n_tp - 1) * rest
-
-            @pl.when(jnp.logical_and(here, t == 0))
-            def _():
-                sent(firsts, (n_tp - 1) * (n_ep - rest), n_ep - 1 - lead)
-
-            @pl.when(jnp.logical_and(here, t > 0))
-            def _():
-                parts = n_ep - lead + (n_tp - 2) * (n_ep - rest)
-                sent(firsts, parts, n_ep - 1 - rest)
 
 
 def local(tokens, chosen, chosen_weight, gate_weight, up_weight, down_weight):
@@ -533,16 +544,16 @@
             dma,
             dma((n_tp,)),
             dma,
-            dma((4,)),
-            dma,
-            dma((n_tp,)),
-            dma,
             dma((GROUPS,)),
             dma,
             dma,
+            dma((GROUPS,)),
+            dma,
+            dma,
             dma,
             dma,
             pltpu.SemaphoreType.REGULAR((n_ep,)),
+            pltpu.SemaphoreType.REGULAR,
             pltpu.SemaphoreType.REGULAR,
             pltpu.SemaphoreType.REGULAR,
         ],

time: 19.5 us -> 19.1 us (0.979)
  the two profiles are of different devices: /device:TPU:9 before, /device:TPU:0 now
where the time goes in v4:
time: 19.1 us; the launch traced here: 18.8 us
  Pallas kernels  18.1 us (95%)
  local copies, waits for them, and re-layouts  0.66 us (3%)
    pallas_call x1, Pallas kernels, local(): pl.pallas_call(functools.partial(kernel, n_ep, n_tp), out_shape=jax.Shape...  18.1 us
    unnamed x1, local copies, waits for them, and re-layouts  0.66 us

profile of v4, /device:TPU:0, one launch (start us, length us, event | category | flops | bytes accessed | tf_op | source)
XLA Modules:
  0.0 18.8 jit_solution(10297829695942556607)
XLA Ops:
  0.0 18.1 %shard_map.64 = bf16[128,512]{1,0:T(8,128)(2,1)S(1)} custom-call(bf16[128,2048]{1,0:T(8,128)(2,1)} %tok_hbm.1, s32[8,8,8]{2,1,0:T(8,128)} %cho_hbm.1, f32[1,8,8]{2,1,0:T(8,128)} %wt_hbm.1, bf16[1,2048,1024]{2,1,0:T(8,128)(2,1)} %gate_hbm.1, bf16[1,2048,1024]{2,1,0:T(8,128)(2,1)} %up_hbm.1, bf16[1,1024,2048]{2,1,0:T(8,128)(2,1)} %down_hbm.1), custom_call_target="tpu_custom_call" | custom-call | tf_op jit(solution)/shard_map/pallas_call | solution.py:520
  18.1 0.7 %copy.8 = bf16[128,512]{1,0:T(8,128)(2,1)} copy(bf16[128,512]{1,0:T(8,128)(2,1)S(1)} %shard_map.64) | data formatting | bytes 262144

commit v5 on v4

--- a/solution.py
+++ b/solution.py
@@ -11,7 +11,7 @@
 GROUPS = 4
 COLUMNS = 4
 FIRST = ((1, 0), (2, 0), (3, 0), (0, 1), (0, 2), (0, 3))
-EVERY = ((2, 0), (3, 0), (3, 1), (0, 2), (0, 3))
+EVERY = ((2, 0), (3, 0), (3, 1), (0, 2), (0, 3), (1, 0))
 SPLIT = (((1, 2), (2, 1)), ((1, 2), (2, 1), (0, 2), (2, 0)))
 EARLY = 2
 
@@ -86,6 +86,11 @@
 
     pl.loop(e + 1, n_ep)(greet)
 
+    @pl.when(mine == GROUPS - 1)
+    def _():
+        each(gs, greet)
+
+
     def greet_tp(p):
         pl.semaphore_signal(barrier, inc=1, device_id={"tp": p}, device_id_type=MESH)
 
@@ -113,7 +118,7 @@
     with jax.named_scope("barrier"):
         floor = e + jnp.minimum(t, 1)
 
-        @pl.when(floor > 0)
+        @pl.when(mine > 0)
         def _():
             pl.semaphore_wait(barrier, floor)
 
@@ -121,9 +126,11 @@
     def answer(p):
         pl.semaphore_signal(ep_ready.at[e], inc=1, device_id={"ep": p}, device_id_type=MESH)
 
-    pl.loop(0, e)(answer)
-
-    @pl.when(t > 0)
+    @pl.when(mine > 0)
+    def _():
+        pl.loop(jnp.where(mine == GROUPS - 1, gs, 0), e)(answer)
+
+    @pl.when(jnp.logical_and(t > 0, mine > 0))
     def _():
         pl.semaphore_signal(tp_seen, inc=1, device_id={"tp": 0}, device_id_type=MESH)
 
@@ -230,7 +237,10 @@
             for k in range(n_tp):
                 send_tokens(k, p).start()
 
-        each(gs - 1, send_near)
+        @pl.when(mine > 0)
+        def _():
+            each(gs - 1, send_near)
+
     with jax.named_scope("hop"):
         for dst in range(1, GROUPS):
             @pl.when(mine == dst - 1)
@@ -240,22 +250,50 @@
                 direct_to(dst)
 
     with jax.named_scope("tpseen"):
-        @pl.when(t == 0)
-        def _():
+        def open_tp():
             pl.semaphore_wait(tp_seen, n_tp - 1)
 
             def admit(p):
                 pl.semaphore_signal(tp_ready, inc=1, device_id={"tp": p}, device_id_type=MESH)
 
             pl.loop(1, n_tp)(admit)
+
+        @pl.when(jnp.logical_and(t == 0, mine > 0))
+        def _():
+            open_tp()
 
     with jax.named_scope("sendup"):
         for dst in range(2, GROUPS):
             @pl.when(mine < dst - 1)
             def _():
-                ready_group(dst)
+                if dst < GROUPS - 1:
+                    ready_group(dst)
+                else:
+                    @pl.when(mine == 0)
+                    def _():
+                        pl.semaphore_wait(barrier, floor + gs)
+
+                    @pl.when(mine > 0)
+                    def _():
+                        ready_group(dst)
+
                 hops_to(dst)
                 direct_to(dst)
+
+        @pl.when(mine == 0)
+        def _():
+            pl.loop(0, e)(answer)
+
+            @pl.when(t > 0)
+            def _():
+                pl.semaphore_signal(tp_seen, inc=1, device_id={"tp": 0}, device_id_type=MESH)
+
+            each(gs - 1, send_near)
+
+            @pl.when(t == 0)
+            def _():
+                open_tp()
+
 
     parts = []
     for x in range(experts):
@@ -264,9 +302,8 @@
         parts.append(jnp.where(position == columns[x], wcol, 0.0))
     weighted = jnp.concatenate(parts, axis=0)
     hi = weighted.astype(jnp.bfloat16).astype(jnp.float32)
-    mid = (weighted - hi).astype(jnp.bfloat16).astype(jnp.float32)
-    lo = weighted - hi - mid
-    place[...] = jnp.concatenate([hi, mid, lo], axis=0).T.astype(jnp.bfloat16)
+    mid = weighted - hi
+    place[...] = jnp.concatenate([hi, mid], axis=0).T.astype(jnp.bfloat16)
 
     def landed(ref, sem):
         pltpu.make_async_copy(ref, ref, sem).wait()
@@ -405,14 +442,14 @@
             for gi in range(EARLY):
                 start_part(i, gi, here)
             for gi in range(EARLY, GROUPS - 1):
-                start_part(i, gi, jnp.logical_and(here, mine != 1))
+                start_part(i, gi, here)
         else:
             for gi in range(GROUPS):
                 start_part(i, gi, here)
         if i == n_tp - 2:
             for gi in range(EARLY, GROUPS):
                 for x in range(n_tp - 1):
-                    late = mine == 1 if gi < GROUPS - 1 else mine > (0 if x == 0 else -1)
+                    late = mine < 0 if gi < GROUPS - 1 else mine > (0 if x == 0 else -1)
                     start_part(x, gi, jnp.logical_and(leaves(x), late))
 
     for gi in range(GROUPS):
@@ -502,7 +539,7 @@
 
     with jax.named_scope("combine"):
         y = back_in[...].astype(jnp.float32).reshape(rows, sw).astype(jnp.bfloat16)
-        y = jnp.concatenate([y, y, y], axis=0)
+        y = jnp.concatenate([y, y], axis=0)
         result = jnp.dot(place[...], y, preferred_element_type=jnp.float32)
         out_ref[...] = result.astype(out_ref.dtype)
 
@@ -533,7 +570,7 @@
             pltpu.VMEM((n_tp, blocks, picks, sw), bf),
             pltpu.VMEM((rows, hid), f32),
             pltpu.VMEM((rows, hid), f32),
-            pltpu.VMEM((tok_count, 3 * experts * picks), bf),
+            pltpu.VMEM((tok_count, 2 * experts * picks), bf),
             pltpu.VMEM((n_tp, blocks, picks, sw), bf),
             pltpu.VMEM((n_tp, blocks, picks, sw), bf),
             pltpu.VMEM((n_tp * n_ep, picks, sw), bf),

time: 19.1 us -> 19.1 us (level)
  no operation moved by 1% of the time
where the time goes in v5:
time: 19.1 us; the launch traced here: 18.7 us
  Pallas kernels  18.1 us (95%)
  local copies, waits for them, and re-layouts  0.66 us (3%)
    pallas_call x1, Pallas kernels, local(): pl.pallas_call(functools.partial(kernel, n_ep, n_tp), out_shape=jax.Shape...  18.1 us
    unnamed x1, local copies, waits for them, and re-layouts  0.66 us

profile of v5, /device:TPU:0, one launch (start us, length us, event | category | flops | bytes accessed | tf_op | source)
XLA Modules:
  0.0 18.7 jit_solution(9288838005798539061)
XLA Ops:
  0.0 18.1 %shard_map.64 = bf16[128,512]{1,0:T(8,128)(2,1)S(1)} custom-call(bf16[128,2048]{1,0:T(8,128)(2,1)} %tok_hbm.1, s32[8,8,8]{2,1,0:T(8,128)} %cho_hbm.1, f32[1,8,8]{2,1,0:T(8,128)} %wt_hbm.1, bf16[1,2048,1024]{2,1,0:T(8,128)(2,1)} %gate_hbm.1, bf16[1,2048,1024]{2,1,0:T(8,128)(2,1)} %up_hbm.1, bf16[1,1024,2048]{2,1,0:T(8,128)(2,1)} %down_hbm.1), custom_call_target="tpu_custom_call" | custom-call | tf_op jit(solution)/shard_map/pallas_call | solution.py:557
  18.1 0.7 %copy.8 = bf16[128,512]{1,0:T(8,128)(2,1)} copy(bf16[128,512]{1,0:T(8,128)(2,1)S(1)} %shard_map.64) | data formatting | bytes 262144

commit v6 on v5

--- a/solution.py
+++ b/solution.py
@@ -99,9 +99,9 @@
         pl.loop(1, n_tp)(greet_tp)
 
     loads = [
-        pltpu.make_async_copy(cho_hbm.at[e], cho, in_sem.at[0]),
-        pltpu.make_async_copy(wt_hbm.at[0], wt, in_sem.at[1]),
-        pltpu.make_async_copy(tok_hbm, tok, in_sem.at[2]),
+        pltpu.make_async_copy(cho_hbm.at[e], cho, in_sem),
+        pltpu.make_async_copy(wt_hbm.at[0], wt, in_sem),
+        pltpu.make_async_copy(tok_hbm, tok, in_sem),
     ]
     for c in loads:
         c.start()
@@ -523,7 +523,7 @@
             come = tuple(sorted(a for a, b in pairs if b == group))
             ends[come] = jnp.logical_or(ends[come], case) if come in ends else case
 
-    for come in sorted(ends):
+    for come in sorted(ends, key=len):
         @pl.when(ends[come])
         def _():
             with jax.named_scope('backin'):
@@ -576,7 +576,7 @@
             pltpu.VMEM((n_tp * n_ep, picks, sw), bf),
             pltpu.VMEM((blocks, picks, sw), bf),
             pltpu.VMEM((experts, picks, sw), bf),
-            dma((3,)),
+            dma,
             dma,
             dma,
             dma((n_tp,)),

time: 19.1 us -> 19 us (level)
  no operation moved by 1% of the time
where the time goes in v6:
time: 19 us; the launch traced here: 18.7 us
  Pallas kernels  18 us (95%)
  local copies, waits for them, and re-layouts  0.66 us (3%)
    pallas_call x1, Pallas kernels, local(): pl.pallas_call(functools.partial(kernel, n_ep, n_tp), out_shape=jax.Shape...  18 us
    unnamed x1, local copies, waits for them, and re-layouts  0.66 us

profile of v6, /device:TPU:0, one launch (start us, length us, event | category | flops | bytes accessed | tf_op | source)
XLA Modules:
  0.0 18.7 jit_solution(13207768772734488824)
XLA Ops:
  0.0 18.0 %shard_map.64 = bf16[128,512]{1,0:T(8,128)(2,1)S(1)} custom-call(bf16[128,2048]{1,0:T(8,128)(2,1)} %tok_hbm.1, s32[8,8,8]{2,1,0:T(8,128)} %cho_hbm.1, f32[1,8,8]{2,1,0:T(8,128)} %wt_hbm.1, bf16[1,2048,1024]{2,1,0:T(8,128)(2,1)} %gate_hbm.1, bf16[1,2048,1024]{2,1,0:T(8,128)(2,1)} %up_hbm.1, bf16[1,1024,2048]{2,1,0:T(8,128)(2,1)} %down_hbm.1), custom_call_target="tpu_custom_call" | custom-call | tf_op jit(solution)/shard_map/pallas_call | solution.py:557
  18.1 0.7 %copy.8 = bf16[128,512]{1,0:T(8,128)(2,1)} copy(bf16[128,512]{1,0:T(8,128)(2,1)S(1)} %shard_map.64) | data formatting | bytes 262144
